TPU v7x, 32 devices: a whole 2x2x4 slice. The times are simulated.
32 devices in a mesh: ep: 8 (over z, y), tp: 4 (over x, core).
Axes of the slice: x: 2, y: 2, z: 4, core: 2. Of those that a mesh axis runs over, the one named last changes fastest.
Arguments:
- tokens: bfloat16 [6144, 2048], P('ep', 'tp')
- norm_gain: float32 [2048], P('tp'), may hold values from 0.1 to 1.9
- routing: int32 [6144, 2], P('ep'), may hold values from 0 to 7, as said below
- route_weight: float32 [6144, 2], P('ep'), may hold values from 0.2 to 1
- w_gate: bfloat16 [8, 2048, 512], P('ep', 'tp'), may hold values from -0.125 to 0.125
- w_up: bfloat16 [8, 2048, 512], P('ep', 'tp'), may hold values from -0.125 to 0.125
- w_down: bfloat16 [8, 512, 2048], P('ep', None, 'tp'), may hold values from -0.25 to 0.25
- w_branch_in: bfloat16 [2048, 1024], P('ep', 'tp'), may hold values from -0.125 to 0.125
- w_branch_out: bfloat16 [1024, 2048], P('tp', 'ep'), may hold values from -0.1875 to 0.1875
- branch_gate: float32 [2048], P('tp'), may hold values from -3 to 3
Outputs:
- mixed: bfloat16 [6144, 2048], P('ep', 'tp')
Inputs may be any that keep to these rules, and one draw needn't show every extreme that they name: `routing`: each row names two different experts of the same group; expert e belongs to group e // 2. Among the rows of one device (aligned blocks of 768 rows) no expert is named more than 384 times, and in every block all experts of one group are named exactly 384 times.
All inputs are finite; a program needn't handle non-finite values.
Results may differ from a plain program's by a relative error of at most 0.0069.
Values may be sent and summed in bfloat16 or wider, within the bound.
A program may use at most 128 MiB of HBM per device.

v0:
```python
import jax
import jax.numpy as jnp
from jax import lax
from jax.sharding import PartitionSpec as P

GROUPS = 4
epsilon = 1e-06


def send_back(result):
    return lax.all_to_all(result, "ep", split_axis=0, concat_axis=0, tiled=True)


def body(
    tokens,
    norm_gain,
    routing,
    route_weight,
    w_gate,
    w_up,
    w_down,
    w_branch_in,
    w_branch_out,
    branch_gate,
):
    token_count, quarter = tokens.shape
    full_width = quarter * lax.axis_size("tp")
    floats = tokens.astype(jnp.float32)
    squares = lax.psum(jnp.sum(floats * floats, axis=1), "tp")
    normed = (floats * lax.rsqrt(squares[:, None] / full_width + epsilon) * norm_gain).astype(
        jnp.bfloat16
    )
    expert_count = lax.axis_size("ep") * w_gate.shape[0]
    capacity = token_count // (expert_count // GROUPS)
    flat_ids = routing.reshape(-1)
    one_hot = (flat_ids[:, None] == jnp.arange(expert_count, dtype=jnp.int32)[None, :]).astype(
        jnp.int32
    )
    before = jnp.cumsum(one_hot, axis=0) - one_hot
    position = flat_ids * capacity + jnp.sum(before * one_hot, axis=1)
    copies = jnp.repeat(normed, 2, axis=0)
    buffer = jnp.zeros((expert_count * capacity, quarter), jnp.bfloat16).at[position].set(copies)
    buffer = buffer.reshape(expert_count, capacity, quarter)
    gate_whole, up_whole, down_whole = (
        lax.all_gather(w_gate[0], "tp", axis=0, tiled=True),
        lax.all_gather(w_up[0], "tp", axis=0, tiled=True),
        lax.all_gather(w_down[0], "tp", axis=1, tiled=True),
    )
    row_split = lax.all_to_all(
        lax.all_to_all(buffer, "ep", split_axis=0, concat_axis=0, tiled=True),
        "tp",
        split_axis=0,
        concat_axis=2,
        tiled=True,
    )
    slot_rows = row_split.reshape(-1, row_split.shape[2])
    gate_sum = jnp.dot(slot_rows, gate_whole, preferred_element_type=jnp.float32)
    up_sum = jnp.dot(slot_rows, up_whole, preferred_element_type=jnp.float32)
    hidden = (jax.nn.silu(gate_sum) * up_sum).astype(jnp.bfloat16)
    result = jnp.dot(hidden, down_whole, preferred_element_type=jnp.float32).astype(jnp.bfloat16)
    feature_split = lax.all_to_all(
        result.reshape(row_split.shape), "tp", split_axis=2, concat_axis=0, tiled=True
    )
    returned = send_back(feature_split)
    picked = returned.reshape(expert_count * capacity, quarter)[position].reshape(
        token_count, 2, quarter
    )
    routed = jnp.sum(picked.astype(jnp.float32) * route_weight[:, :, None], axis=1)
    branch_tokens = lax.all_to_all(normed, "tp", split_axis=0, concat_axis=1, tiled=True)
    in_cols, out_rows = (
        lax.all_gather(w_branch_in, "tp", axis=1, tiled=True),
        lax.all_gather(w_branch_out, "tp", axis=0, tiled=True),
    )
    in_whole, out_whole = (
        lax.all_gather(in_cols, "ep", axis=0, tiled=True),
        lax.all_gather(out_rows, "ep", axis=1, tiled=True),
    )
    branch_hidden = jax.nn.silu(
        jnp.dot(branch_tokens, in_whole, preferred_element_type=jnp.float32)
    ).astype(jnp.bfloat16)
    branch_local = jnp.dot(branch_hidden, out_whole, preferred_element_type=jnp.float32).astype(
        jnp.bfloat16
    )
    branch = lax.all_to_all(branch_local, "tp", split_axis=1, concat_axis=0, tiled=True)
    return (routed + jax.nn.sigmoid(branch_gate) * branch.astype(jnp.float32)).astype(jnp.bfloat16)


def solution(mesh):
    return jax.shard_map(
        body,
        mesh=mesh,
        in_specs=(
            P("ep", "tp"),
            P("tp"),
            P("ep", None),
            P("ep", None),
            P("ep", "tp", None),
            P("ep", "tp", None),
            P("ep", None, "tp"),
            P("ep", "tp"),
            P("tp", "ep"),
            P("tp"),
        ),
        out_specs=P("ep", "tp"),
        check_vma=False,
    )
```

profile of v0, /device:TPU:0, one launch (start us, length us, event | category | flops | bytes accessed | tf_op | source)
XLA Modules:
  0.0 403.0 jit_solution(17927686198045265100)
XLA Ops:
  10.8 8.4 %psum.7 = f32[768]{0:T(1024)S(1)} all-reduce(f32[768]{0:T(1024)S(1)} %fusion.5), channel_id=1, replica_groups=mesh['ep'=8,'tp'=4] {'tp'}, use_global_device_ids=true, to_apply=%region_4.5 | all-reduce | flops 768 | bytes 6144 | tf_op jit(solution)/shard_map/psum | solution.py:29
  19.2 2.3 reduce-window.6
  25.4 9.5 %scatter_custom_fusion = bf16[3072,512]{1,0:T(8,128)(2,1)} fusion(s32[1536]{0:T(1024)S(1)} %fusion.21, bf16[1536,512]{1,0:T(8,128)(2,1)S(1)} %reshape.100, bf16[]{:T(256)} %constant.8.clone.1), kind=kCustom, calls=%fused_computation.19 | custom fusion | bytes 3145730 | tf_op jit(solution)/shard_map/scatter | solution.py:42
  34.8 6.0 %all-to-all-start = ((bf16[8,384,512]{2,1,0:T(8,128)(2,1)}), bf16[8,384,512]{2,1,0:T(8,128)(2,1)S(1)}, u32[]{:S(2)}, u32[]{:S(2)}) async-start(bf16[8,384,512]{2,1,0:T(8,128)(2,1)} %bitcast.69), calls=%async_computation | async-start | bytes 6291456 | tf_op jit(solution)/shard_map/all_to_all | solution.py:50
  40.8 8.6 %all_gather.26 = bf16[1024,256]{1,0:T(8,128)(2,1)} all-gather(bf16[256,256]{1,0:T(8,128)(2,1)S(1)} %copy-done.2), channel_id=1, replica_groups=mesh['ep'=8,'tp'=4] {'tp'}, dimensions={0}, use_global_device_ids=true | all-gather | bytes 655360 | tf_op jit(solution)/shard_map/all_gather | solution.py:72
  49.5 75.0 %all-to-all-done = bf16[8,384,512]{2,1,0:T(8,128)(2,1)S(1)} async-done(((bf16[8,384,512]{2,1,0:T(8,128)(2,1)}), bf16[8,384,512]{2,1,0:T(8,128)(2,1)S(1)}, u32[]{:S(2)}, u32[]{:S(2)}) %all-to-all-start) | async-done | bytes 3145760 | tf_op jit(solution)/shard_map/all_to_all | solution.py:50
  124.5 39.5 %all_to_all.75 = bf16[8,384,512]{2,1,0:T(8,128)(2,1)S(1)} all-to-all(bf16[8,384,512]{2,1,0:T(8,128)(2,1)S(1)} %all-to-all-done), channel_id=1, replica_groups=mesh['ep'=8,'tp'=4] {'tp'}, dimensions={0} | all-to-all | bytes 6291456 | tf_op jit(solution)/shard_map/all_to_all | solution.py:49
  164.0 2.4 copy.32
  167.5 4.5 %fusion.3 = f32[768,512]{1,0:T(8,128)} fusion(bf16[768,2048]{1,0:T(8,128)(2,1)S(1)} %bitcast.73, bf16[1,2048,512]{2,1,0:T(8,128)(2,1)} %all-gather.13.cloned.1.call-done), kind=kOutput, calls=%fused_computation.8 | convolution fusion | flops 1610612736 | bytes 6815744 | tf_op jit(solution)/shard_map/dot_general | solution.py:57
  172.0 7.9 %convolution_convert_fusion = bf16[768,2048]{1,0:T(8,128)(2,1)} fusion(bf16[1,512,2048]{2,1,0:T(8,128)(2,1)} %all-gather.17.cloned.1.call-done, f32[768,512]{1,0:T(8,128)} %fusion.3, bf16[768,2048]{1,0:T(8,128)(2,1)S(1)} %bitcast.74, bf16[1,2048,512]{2,1,0:T(8,128)(2,1)} %all-gather.15.cloned.1.call-done), kind=kOutput, calls=%fused_computation.2 | convolution fusion | flops 3225157632 | bytes 12058624 | tf_op jit(solution)/shard_map/dot_general | solution.py:60
  179.9 8.8 %copy.33 = bf16[2,384,2048]{1,0,2:T(2,128)(2,1)} copy(bf16[2,384,2048]{2,1,0:T(8,128)(2,1)} %bitcast.75) | data formatting | bytes 6291456 | tf_op jit(solution)/shard_map/reshape | solution.py:62
  188.6 3.8 all-to-all-start.2
  192.5 40.9 %all_gather.24 = bf16[256,1024]{1,0:T(8,128)(2,1)} all-gather(bf16[256,256]{1,0:T(8,128)(2,1)S(1)} %copy-done.3), channel_id=1, replica_groups=mesh['ep'=8,'tp'=4] {'tp'}, dimensions={1}, use_global_device_ids=true | all-gather | bytes 655360 | tf_op jit(solution)/shard_map/all_gather | solution.py:71
  233.5 4.2 %all-to-all-start.4 = ((bf16[4,192,512]{2,1,0:T(8,128)(2,1)}), bf16[4,192,512]{2,1,0:T(8,128)(2,1)}, u32[]{:S(2)}, u32[]{:S(2)}) async-start(bf16[4,192,512]{2,1,0:T(8,128)(2,1)} %bitcast.72), calls=%async_computation.4 | async-start | bytes 1572864 | tf_op jit(solution)/shard_map/all_to_all | solution.py:69
  237.7 6.7 %copy.34 = bf16[4,2,384,512]{3,2,1,0:T(8,128)(2,1)} copy(bf16[4,2,384,512]{2,1,3,0:T(2,128)(2,1)S(1)} %bitcast.68) | data formatting | bytes 6291456 | tf_op jit(solution)/shard_map/all_to_all | solution.py:61
  244.4 5.0 %all-to-all-done.4 = bf16[4,192,512]{2,1,0:T(8,128)(2,1)} async-done(((bf16[4,192,512]{2,1,0:T(8,128)(2,1)}), bf16[4,192,512]{2,1,0:T(8,128)(2,1)}, u32[]{:S(2)}, u32[]{:S(2)}) %all-to-all-start.4) | async-done | bytes 786464 | tf_op jit(solution)/shard_map/all_to_all | solution.py:69
  249.4 6.3 %all-to-all-start.3 = ((bf16[8,384,512]{2,1,0:T(8,128)(2,1)}), bf16[8,384,512]{2,1,0:T(8,128)(2,1)S(1)}, u32[]{:S(2)}, u32[]{:S(2)}) async-start(bf16[8,384,512]{2,1,0:T(8,128)(2,1)} %bitcast.67), calls=%async_computation.3 | async-start | bytes 6291456 | tf_op jit(solution)/shard_map/all_to_all | solution.py:11
  257.8 107.4 %all-gather.9.cloned.1.call-done = bf16[2048,1024]{1,0:T(8,128)(2,1)} async-done(((bf16[256,1024]{1,0:T(8,128)(2,1)}), bf16[2048,1024]{1,0:T(8,128)(2,1)}) %all-gather.9.cloned.1.call-update) | async-done | bytes 4194320 | tf_op jit(solution)/shard_map/all_gather | solution.py:75
  365.2 6.4 %convolution_convert_fusion.1 = bf16[192,2048]{1,0:T(8,128)(2,1)} fusion(bf16[1024,2048]{1,0:T(8,128)(2,1)} %all-gather.11.cloned.1.call-done, bf16[192,2048]{1,0:T(8,128)(2,1)} %bitcast.77, bf16[2048,1024]{1,0:T(8,128)(2,1)} %all-gather.9.cloned.1.call-done), kind=kOutput, calls=%fused_computation.4 | convolution fusion | flops 1611988992 | bytes 9961472 | tf_op jit(solution)/shard_map/dot_general | solution.py:81
  373.8 4.4 %all-to-all-start.5 = ((bf16[192,4,512]{2,0,1:T(8,128)(2,1)}), bf16[192,4,512]{2,0,1:T(8,128)(2,1)}, u32[]{:S(2)}, u32[]{:S(2)}) async-start(bf16[192,4,512]{2,0,1:T(8,128)(2,1)} %bitcast.76), calls=%async_computation.5 | async-start | bytes 1572864 | tf_op jit(solution)/shard_map/all_to_all | solution.py:84
  379.0 5.4 %gather_fusion = bf16[1536,512]{1,0:T(8,128)(2,1)} fusion(bf16[3072,512]{1,0:T(8,128)(2,1)S(1)} %bitcast.66, s32[2048]{0:T(1024)S(1)} %pad_clamp_fusion), kind=kCustom, calls=%fused_computation | custom fusion | bytes 3151872 | tf_op jit(solution)/shard_map/gather | solution.py:65
  384.4 3.4 reshape.86
  387.8 5.9 %multiply_reduce_fusion = f32[768,512]{1,0:T(8,128)} fusion(f32[768,2,512]{2,1,0:T(2,128)S(1)} %reshape.86, f32[768,2]{1,0:T(8,128)S(1)} %copy.35), kind=kLoop, calls=%fused_computation.3 | loop fusion | flops 1179648 | bytes 4724736 | tf_op jit(solution)/shard_map/reduce_sum | solution.py:68
  393.8 2.7 fusion.9
  (56 shorter events, 14.2 us)
Async XLA Ops:
  6.5 4.0 %copy-start.1 = (bf16[768,512]{1,0:T(8,128)(2,1)S(1)}, bf16[768,512]{1,0:T(8,128)(2,1)}, u32[]{:S(2)}) copy-start(bf16[768,512]{1,0:T(8,128)(2,1)} %param.10) | copy-start | bytes 2359300
  6.5 160.9 %all-gather.13.cloned.1.call-start = ((), (), s32[]{:S(2)}) async-start(), calls=%async_computation.8 | async-start | bytes 2621440 | tf_op jit(solution)/shard_map/all_gather | solution.py:45
  7.3 15.3 %copy-start.6 = (f32[512]{0:T(512)S(1)}, f32[512]{0:T(512)}, u32[]{:S(2)}) copy-start(f32[512]{0:T(512)} %param.11) | copy-start | bytes 6148
  7.3 164.7 %all-gather.15.cloned.1.call-start = ((), (), s32[]{:S(2)}) async-start(), calls=%async_computation.9 | async-start | bytes 2621440 | tf_op jit(solution)/shard_map/all_gather | solution.py:46
  8.0 164.0 %all-gather.17.cloned.1.call-start = ((), (), s32[]{:S(2)}) async-start(), calls=%async_computation.10 | async-start | bytes 2621440 | tf_op jit(solution)/shard_map/all_gather | solution.py:47
  22.9 0.9 copy-start
  34.8 6.0 %copy-start.2 = (bf16[256,256]{1,0:T(8,128)(2,1)S(1)}, bf16[256,256]{1,0:T(8,128)(2,1)}, u32[]{:S(2)}) copy-start(bf16[256,256]{1,0:T(8,128)(2,1)} %param.18) | copy-start | bytes 393220
  34.8 89.7 %all-to-all-start = ((bf16[8,384,512]{2,1,0:T(8,128)(2,1)}), bf16[8,384,512]{2,1,0:T(8,128)(2,1)S(1)}, u32[]{:S(2)}, u32[]{:S(2)}) async-start(bf16[8,384,512]{2,1,0:T(8,128)(2,1)} %bitcast.69), calls=%async_computation | async-start | bytes 6291456 | tf_op jit(solution)/shard_map/all_to_all | solution.py:50
  40.8 217.0 %all-gather.11.cloned.1.call-start = ((), (), s32[]{:S(2)}) async-start(), calls=%async_computation.7 | async-start | bytes 4718592 | tf_op jit(solution)/shard_map/all_gather | solution.py:76
  188.6 3.9 copy-start.3
  188.6 44.9 %all-to-all-start.2 = ((bf16[2,384,2048]{1,0,2:T(2,128)(2,1)}), bf16[2,384,2048]{1,0,2:T(2,128)(2,1)S(1)}, u32[]{:S(2)}, u32[]{:S(2)}) async-start(bf16[2,384,2048]{1,0,2:T(2,128)(2,1)} %copy.33), calls=%async_computation.2 | async-start | bytes 6291456 | tf_op jit(solution)/shard_map/all_to_all | solution.py:61
  192.5 172.7 %all-gather.9.cloned.1.call-start = ((), (), s32[]{:S(2)}) async-start(), calls=%async_computation.6 | async-start | bytes 4718592 | tf_op jit(solution)/shard_map/all_gather | solution.py:75
  233.5 15.9 %all-to-all-start.4 = ((bf16[4,192,512]{2,1,0:T(8,128)(2,1)}), bf16[4,192,512]{2,1,0:T(8,128)(2,1)}, u32[]{:S(2)}, u32[]{:S(2)}) async-start(bf16[4,192,512]{2,1,0:T(8,128)(2,1)} %bitcast.72), calls=%async_computation.4 | async-start | bytes 1572864 | tf_op jit(solution)/shard_map/all_to_all | solution.py:69
  249.4 124.4 %all-to-all-start.3 = ((bf16[8,384,512]{2,1,0:T(8,128)(2,1)}), bf16[8,384,512]{2,1,0:T(8,128)(2,1)S(1)}, u32[]{:S(2)}, u32[]{:S(2)}) async-start(bf16[8,384,512]{2,1,0:T(8,128)(2,1)} %bitcast.67), calls=%async_computation.3 | async-start | bytes 6291456 | tf_op jit(solution)/shard_map/all_to_all | solution.py:11
  371.7 6.6 %copy-start.7 = (f32[512]{0:T(512)S(1)}, f32[512]{0:T(512)}, u32[]{:S(2)}) copy-start(f32[512]{0:T(512)} %param.19) | copy-start | bytes 6148
  371.7 7.2 %copy-start.5 = (f32[768,2]{0,1:T(2,128)S(1)}, f32[768,2]{0,1:T(2,128)}, u32[]{:S(2)}) copy-start(f32[768,2]{0,1:T(2,128)} %param.13) | copy-start | bytes 18436
  373.8 20.0 %all-to-all-start.5 = ((bf16[192,4,512]{2,0,1:T(8,128)(2,1)}), bf16[192,4,512]{2,0,1:T(8,128)(2,1)}, u32[]{:S(2)}, u32[]{:S(2)}) async-start(bf16[192,4,512]{2,0,1:T(8,128)(2,1)} %bitcast.76), calls=%async_computation.5 | async-start | bytes 1572864 | tf_op jit(solution)/shard_map/all_to_all | solution.py:84
  387.8 5.9 %copy-start.4 = (f32[512]{0:T(512)S(1)}, f32[512]{0:T(512)}, u32[]{:S(2)}) copy-start(f32[512]{0:T(512)} %add_divide_fusion) | copy-start | bytes 6148
Sparse Core Ops, SparseCore 0:
  8.9 25.2 all-gather.12
  35.8 23.4 all-gather.14
  60.8 23.6 all-gather.16
  86.4 92.0 all-gather.10
  233.6 131.5 all-gather.8
where the time goes:
time: 404 us; the launch traced here: 403 us
  waiting for transfers between devices  190 us (47%)
  blocking collectives  97.4 us (24%)
  local copies, waits for them, and re-layouts  46 us (11%)
  starting transfers between devices  24.9 us (6%)
  matrix products  18.9 us (5%)
  between operations  13.4 us (3%)
  other arithmetic  13 us (3%)
    all_gather x1, waiting for transfers between devices, body(): lax.all_gather(in_cols, 'ep', axis=0, tiled=True)  107 us
    all_to_all x1, waiting for transfers between devices, body(): lax.all_to_all(buffer, 'ep', split_axis=0, concat_axis=0, tiled=True)  75 us
    all_gather x1, blocking collectives, body(): lax.all_gather(w_branch_in, 'tp', axis=1, tiled=True)  40.9 us
    all_to_all x1, blocking collectives, body(): lax.all_to_all(lax.all_to_all(buffer, 'ep', split_axis=0, concat_axis=0,...  39.5 us
    scatter x1, local copies, waits for them, and re-layouts, body(): jnp.zeros((expert_count * capacity, quarter), jnp.bfloat16).at[position]  9.46 us
    reshape x1, local copies, waits for them, and re-layouts, body(): result.reshape(row_split.shape)  8.75 us
    all_gather x1, blocking collectives, body(): lax.all_gather(w_branch_out, 'tp', axis=0, tiled=True)  8.6 us
    psum x1, blocking collectives, body(): squares = lax.psum(jnp.sum(floats * floats, axis=1), 'tp')  8.37 us
  transfers between devices with their start and end apart: 10, of which 3 were waited for; matrix products, arithmetic and copies ran while one was open for 18% of the time, Pallas kernels for 0%

commit v1 on v0

--- a/solution.py
+++ b/solution.py
@@ -68,7 +68,9 @@
     routed = jnp.sum(picked.astype(jnp.float32) * route_weight[:, :, None], axis=1)
     branch_tokens = lax.all_to_all(normed, "tp", split_axis=0, concat_axis=1, tiled=True)
     in_cols, out_rows = (
-        lax.all_gather(w_branch_in, "tp", axis=1, tiled=True),
+        jnp.concatenate(
+            lax.all_to_all(jnp.stack([w_branch_in] * lax.axis_size("tp")), "tp", 0, 0), axis=1
+        ),
         lax.all_gather(w_branch_out, "tp", axis=0, tiled=True),
     )
     in_whole, out_whole = (

time: 404 us -> 374 us (0.926)
  blocking collectives: 97.4 us -> 17.1 us
  waiting for transfers between devices: 190 us -> 230 us
  starting transfers between devices: 24.9 us -> 32.7 us
    all_gather x1, waiting for transfers between devices: 107 us -> 41.1 us  [body(): lax.all_gather(in_cols, 'ep', axis=0, tiled=True)]
    all_gather x1 -> x0, blocking collectives: 40.9 us -> none  [body(): lax.all_gather(w_branch_in, 'tp', axis=1, tiled=True)]
    all_to_all x1 -> x0, blocking collectives: 39.5 us -> none  [body(): lax.all_to_all(lax.all_to_all(buffer, 'ep', split_axis=0, concat_axis=0,...]
    all_to_all x0 -> x2, waiting for transfers between devices: none -> 36.8 us  [the longest x1 36.8 us: body(): lax.all_to_all(lax.all_to_all(buffer, 'ep', split_axis=0, concat_axis=0,...]
    all_to_all x1, waiting for transfers between devices: 0.01 us -> 36.3 us  [body(): lax.all_to_all(result.reshape(row_split.shape), 'tp', split_axis=2, conca...]
    all_to_all x1, waiting for transfers between devices: 0.01 us -> 33.7 us  [send_back(): return lax.all_to_all(result, 'ep', split_axis=0, concat_axis=0, tiled=True)]
    all_to_all x0 -> x2, starting transfers between devices: none -> 8.03 us  [the longest x1 4.31 us: body(): lax.all_to_all(jnp.stack([w_branch_in] * lax.axis_size('tp')), 'tp', 0, 0)]
  transfers between devices with their start and end apart: 10 -> 12, of which waited for: 3 -> 6; matrix products, arithmetic and copies ran while one was open for 18% -> 20% of each run, Pallas kernels for 0% -> 0%
where the time goes in v1:
time: 374 us; the launch traced here: 373 us
  waiting for transfers between devices  230 us (61%)
  local copies, waits for them, and re-layouts  47.1 us (13%)
  starting transfers between devices  32.7 us (9%)
  matrix products  19.5 us (5%)
  blocking collectives  17.1 us (5%)
  between operations  13.4 us (4%)
  other arithmetic  13 us (3%)
    all_to_all x1, waiting for transfers between devices, body(): lax.all_to_all(buffer, 'ep', split_axis=0, concat_axis=0, tiled=True)  75 us
    all_gather x1, waiting for transfers between devices, body(): lax.all_gather(in_cols, 'ep', axis=0, tiled=True)  41.1 us
    all_to_all x1, waiting for transfers between devices, body(): lax.all_to_all(lax.all_to_all(buffer, 'ep', split_axis=0, concat_axis=0,...  36.8 us
    all_to_all x1, waiting for transfers between devices, body(): lax.all_to_all(result.reshape(row_split.shape), 'tp', split_axis=2, conca...  36.3 us
    all_to_all x1, waiting for transfers between devices, send_back(): return lax.all_to_all(result, 'ep', split_axis=0, concat_axis=0, tiled=True)  33.7 us
    scatter x1, local copies, waits for them, and re-layouts, body(): jnp.zeros((expert_count * capacity, quarter), jnp.bfloat16).at[position]  9.5 us
    reshape x1, local copies, waits for them, and re-layouts, body(): result.reshape(row_split.shape)  8.85 us
    all_gather x1, blocking collectives, body(): lax.all_gather(w_branch_out, 'tp', axis=0, tiled=True)  8.69 us
  transfers between devices with their start and end apart: 12, of which 6 were waited for; matrix products, arithmetic and copies ran while one was open for 20% of the time, Pallas kernels for 0%

profile of v1, /device:TPU:0, one launch (start us, length us, event | category | flops | bytes accessed | tf_op | source)
XLA Modules:
  0.0 373.3 jit_solution(15003782295661667089)
XLA Ops:
  10.8 8.4 %psum.7 = f32[768]{0:T(1024)S(1)} all-reduce(f32[768]{0:T(1024)S(1)} %fusion.5), channel_id=1, replica_groups=mesh['ep'=8,'tp'=4] {'tp'}, use_global_device_ids=true, to_apply=%region_4.5 | all-reduce | flops 768 | bytes 6144 | tf_op jit(solution)/shard_map/psum | solution.py:29
  25.4 9.5 %scatter_custom_fusion = bf16[3072,512]{1,0:T(8,128)(2,1)} fusion(s32[1536]{0:T(1024)S(1)} %fusion.21, bf16[1536,512]{1,0:T(8,128)(2,1)S(1)} %reshape.110, bf16[]{:T(256)} %constant.8.clone.1), kind=kCustom, calls=%fused_computation.19 | custom fusion | bytes 3145730 | tf_op jit(solution)/shard_map/scatter | solution.py:42
  34.9 6.0 %all-to-all-start = ((bf16[8,384,512]{2,1,0:T(8,128)(2,1)}), bf16[8,384,512]{2,1,0:T(8,128)(2,1)}, u32[]{:S(2)}, u32[]{:S(2)}) async-start(bf16[8,384,512]{2,1,0:T(8,128)(2,1)} %bitcast.1), calls=%async_computation | async-start | bytes 6291456 | tf_op jit(solution)/shard_map/all_to_all | solution.py:50
  40.9 8.7 %all_gather.22 = bf16[1024,256]{1,0:T(8,128)(2,1)} all-gather(bf16[256,256]{1,0:T(8,128)(2,1)S(1)} %copy-done.2), channel_id=1, replica_groups=mesh['ep'=8,'tp'=4] {'tp'}, dimensions={0}, use_global_device_ids=true | all-gather | bytes 655360 | tf_op jit(solution)/shard_map/all_gather | solution.py:74
  49.6 75.0 %all-to-all-done = bf16[8,384,512]{2,1,0:T(8,128)(2,1)} async-done(((bf16[8,384,512]{2,1,0:T(8,128)(2,1)}), bf16[8,384,512]{2,1,0:T(8,128)(2,1)}, u32[]{:S(2)}, u32[]{:S(2)}) %all-to-all-start) | async-done | bytes 3145760 | tf_op jit(solution)/shard_map/all_to_all | solution.py:50
  124.6 3.7 all-to-all-start.1
  128.5 36.8 %all-to-all-done.1 = bf16[8,384,512]{2,1,0:T(8,128)(2,1)S(1)} async-done(((bf16[8,384,512]{2,1,0:T(8,128)(2,1)}), bf16[8,384,512]{2,1,0:T(8,128)(2,1)S(1)}, u32[]{:S(2)}, u32[]{:S(2)}) %all-to-all-start.1) | async-done | bytes 3145760 | tf_op jit(solution)/shard_map/all_to_all | solution.py:49
  166.1 4.3 %all-to-all-start.5 = ((bf16[4,256,256]{1,2,0:T(8,128)(2,1)}), bf16[4,256,256]{1,2,0:T(8,128)(2,1)}, u32[]{:S(2)}, u32[]{:S(2)}) async-start(bf16[4,256,256]{1,2,0:T(8,128)(2,1)} %stack.2), calls=%async_computation.5 | async-start | bytes 1048576 | tf_op jit(solution)/shard_map/all_to_all | solution.py:72
  173.9 4.6 %fusion.3 = f32[768,512]{1,0:T(8,128)} fusion(bf16[768,2048]{1,0:T(8,128)(2,1)S(1)} %bitcast.75, bf16[1,2048,512]{2,1,0:T(8,128)(2,1)} %all-gather.13.cloned.1.call-done), kind=kOutput, calls=%fused_computation.8 | convolution fusion | flops 1610612736 | bytes 6815744 | tf_op jit(solution)/shard_map/dot_general | solution.py:57
  178.5 7.9 %convolution_convert_fusion = bf16[768,2048]{1,0:T(8,128)(2,1)} fusion(bf16[1,512,2048]{2,1,0:T(8,128)(2,1)} %all-gather.17.cloned.1.call-done, f32[768,512]{1,0:T(8,128)} %fusion.3, bf16[768,2048]{1,0:T(8,128)(2,1)S(1)} %bitcast.76, bf16[1,2048,512]{2,1,0:T(8,128)(2,1)} %all-gather.15.cloned.1.call-done), kind=kOutput, calls=%fused_computation.2 | convolution fusion | flops 3225157632 | bytes 12058624 | tf_op jit(solution)/shard_map/dot_general | solution.py:60
  186.4 8.9 %copy.35 = bf16[2,384,2048]{1,0,2:T(2,128)(2,1)} copy(bf16[2,384,2048]{2,1,0:T(8,128)(2,1)} %bitcast.77) | data formatting | bytes 6291456 | tf_op jit(solution)/shard_map/reshape | solution.py:62
  195.3 3.7 all-to-all-start.2
  199.6 36.3 %all-to-all-done.2 = bf16[2,384,2048]{1,0,2:T(2,128)(2,1)S(1)} async-done(((bf16[2,384,2048]{1,0,2:T(2,128)(2,1)}), bf16[2,384,2048]{1,0,2:T(2,128)(2,1)S(1)}, u32[]{:S(2)}, u32[]{:S(2)}) %all-to-all-start.2) | async-done | bytes 3145760 | tf_op jit(solution)/shard_map/all_to_all | solution.py:61
  235.9 4.2 %all-to-all-start.4 = ((bf16[4,192,512]{2,1,0:T(8,128)(2,1)}), bf16[4,192,512]{2,1,0:T(8,128)(2,1)}, u32[]{:S(2)}, u32[]{:S(2)}) async-start(bf16[4,192,512]{2,1,0:T(8,128)(2,1)} %bitcast.74), calls=%async_computation.4 | async-start | bytes 1572864 | tf_op jit(solution)/shard_map/all_to_all | solution.py:69
  240.1 6.7 %copy.36 = bf16[4,2,384,512]{3,2,1,0:T(8,128)(2,1)} copy(bf16[4,2,384,512]{2,1,3,0:T(2,128)(2,1)S(1)} %bitcast.71) | data formatting | bytes 6291456 | tf_op jit(solution)/shard_map/all_to_all | solution.py:61
  246.8 5.0 %all-to-all-done.4 = bf16[4,192,512]{2,1,0:T(8,128)(2,1)} async-done(((bf16[4,192,512]{2,1,0:T(8,128)(2,1)}), bf16[4,192,512]{2,1,0:T(8,128)(2,1)}, u32[]{:S(2)}, u32[]{:S(2)}) %all-to-all-start.4) | async-done | bytes 786464 | tf_op jit(solution)/shard_map/all_to_all | solution.py:69
  251.7 6.3 %all-to-all-start.3 = ((bf16[8,384,512]{2,1,0:T(8,128)(2,1)}), bf16[8,384,512]{2,1,0:T(8,128)(2,1)S(1)}, u32[]{:S(2)}, u32[]{:S(2)}) async-start(bf16[8,384,512]{2,1,0:T(8,128)(2,1)} %bitcast.70), calls=%async_computation.3 | async-start | bytes 6291456 | tf_op jit(solution)/shard_map/all_to_all | solution.py:11
  260.1 41.1 %all-gather.9.cloned.1.call-done = bf16[2048,1024]{0,1:T(8,128)(2,1)} async-done(((bf16[256,1024]{0,1:T(8,128)(2,1)}), bf16[2048,1024]{0,1:T(8,128)(2,1)}) %all-gather.9.cloned.1.call-update) | async-done | bytes 4194320 | tf_op jit(solution)/shard_map/all_gather | solution.py:77
  301.2 7.0 %convolution_convert_fusion.1 = bf16[192,2048]{1,0:T(8,128)(2,1)} fusion(bf16[1024,2048]{1,0:T(8,128)(2,1)} %all-gather.11.cloned.1.call-done, bf16[192,2048]{1,0:T(8,128)(2,1)} %bitcast.79, bf16[2048,1024]{0,1:T(8,128)(2,1)} %all-gather.9.cloned.1.call-done), kind=kOutput, calls=%fused_computation.4 | convolution fusion | flops 1611988992 | bytes 9961472 | tf_op jit(solution)/shard_map/dot_general | solution.py:83
  310.3 33.7 %all-to-all-done.3 = bf16[8,384,512]{2,1,0:T(8,128)(2,1)S(1)} async-done(((bf16[8,384,512]{2,1,0:T(8,128)(2,1)}), bf16[8,384,512]{2,1,0:T(8,128)(2,1)S(1)}, u32[]{:S(2)}, u32[]{:S(2)}) %all-to-all-start.3) | async-done | bytes 3145760 | tf_op jit(solution)/shard_map/all_to_all | solution.py:11
  344.0 4.4 %all-to-all-start.6 = ((bf16[192,4,512]{2,0,1:T(8,128)(2,1)}), bf16[192,4,512]{2,0,1:T(8,128)(2,1)}, u32[]{:S(2)}, u32[]{:S(2)}) async-start(bf16[192,4,512]{2,0,1:T(8,128)(2,1)} %bitcast.78), calls=%async_computation.6 | async-start | bytes 1572864 | tf_op jit(solution)/shard_map/all_to_all | solution.py:86
  349.2 5.4 %gather_fusion = bf16[1536,512]{1,0:T(8,128)(2,1)} fusion(bf16[3072,512]{1,0:T(8,128)(2,1)S(1)} %bitcast.69, s32[2048]{0:T(1024)S(1)} %pad_clamp_fusion), kind=kCustom, calls=%fused_computation | custom fusion | bytes 3151872 | tf_op jit(solution)/shard_map/gather | solution.py:65
  354.6 3.4 reshape.96
  358.1 5.9 %multiply_reduce_fusion = f32[768,512]{1,0:T(8,128)} fusion(f32[768,2,512]{2,1,0:T(2,128)S(1)} %reshape.96, f32[768,2]{1,0:T(8,128)S(1)} %copy.37), kind=kLoop, calls=%fused_computation.3 | loop fusion | flops 1179648 | bytes 4724736 | tf_op jit(solution)/shard_map/reduce_sum | solution.py:68
  (60 shorter events, 23.1 us)
Async XLA Ops:
  6.5 4.0 %copy-start.1 = (bf16[768,512]{1,0:T(8,128)(2,1)S(1)}, bf16[768,512]{1,0:T(8,128)(2,1)}, u32[]{:S(2)}) copy-start(bf16[768,512]{1,0:T(8,128)(2,1)} %param.10) | copy-start | bytes 2359300
  6.5 167.3 %all-gather.13.cloned.1.call-start = ((), (), s32[]{:S(2)}) async-start(), calls=%async_computation.9 | async-start | bytes 2621440 | tf_op jit(solution)/shard_map/all_gather | solution.py:45
  7.3 15.3 %copy-start.6 = (f32[512]{0:T(512)S(1)}, f32[512]{0:T(512)}, u32[]{:S(2)}) copy-start(f32[512]{0:T(512)} %param.11) | copy-start | bytes 6148
  7.3 171.3 %all-gather.15.cloned.1.call-start = ((), (), s32[]{:S(2)}) async-start(), calls=%async_computation.10 | async-start | bytes 2621440 | tf_op jit(solution)/shard_map/all_gather | solution.py:46
  8.0 170.5 %all-gather.17.cloned.1.call-start = ((), (), s32[]{:S(2)}) async-start(), calls=%async_computation.11 | async-start | bytes 2621440 | tf_op jit(solution)/shard_map/all_gather | solution.py:47
  22.9 0.9 copy-start
  34.9 6.0 %copy-start.2 = (bf16[256,256]{1,0:T(8,128)(2,1)S(1)}, bf16[256,256]{1,0:T(8,128)(2,1)}, u32[]{:S(2)}) copy-start(bf16[256,256]{1,0:T(8,128)(2,1)} %param.18) | copy-start | bytes 393220
  34.9 89.8 %all-to-all-start = ((bf16[8,384,512]{2,1,0:T(8,128)(2,1)}), bf16[8,384,512]{2,1,0:T(8,128)(2,1)}, u32[]{:S(2)}, u32[]{:S(2)}) async-start(bf16[8,384,512]{2,1,0:T(8,128)(2,1)} %bitcast.1), calls=%async_computation | async-start | bytes 6291456 | tf_op jit(solution)/shard_map/all_to_all | solution.py:50
  40.8 219.3 %all-gather.11.cloned.1.call-start = ((), (), s32[]{:S(2)}) async-start(), calls=%async_computation.8 | async-start | bytes 4718592 | tf_op jit(solution)/shard_map/all_gather | solution.py:78
  49.6 78.8 %copy-start.3 = (bf16[256,256]{1,0:T(8,128)(2,1)S(1)}, bf16[256,256]{1,0:T(8,128)(2,1)}, u32[]{:S(2)}) copy-start(bf16[256,256]{1,0:T(8,128)(2,1)} %param.17) | copy-start | bytes 393220
  124.6 40.6 %all-to-all-start.1 = ((bf16[8,384,512]{2,1,0:T(8,128)(2,1)}), bf16[8,384,512]{2,1,0:T(8,128)(2,1)S(1)}, u32[]{:S(2)}, u32[]{:S(2)}) async-start(bf16[8,384,512]{2,1,0:T(8,128)(2,1)} %all-to-all-done), calls=%async_computation.1 | async-start | bytes 6291456 | tf_op jit(solution)/shard_map/all_to_all | solution.py:49
  166.1 29.2 %all-to-all-start.5 = ((bf16[4,256,256]{1,2,0:T(8,128)(2,1)}), bf16[4,256,256]{1,2,0:T(8,128)(2,1)}, u32[]{:S(2)}, u32[]{:S(2)}) async-start(bf16[4,256,256]{1,2,0:T(8,128)(2,1)} %stack.2), calls=%async_computation.5 | async-start | bytes 1048576 | tf_op jit(solution)/shard_map/all_to_all | solution.py:72
  195.3 40.6 %all-to-all-start.2 = ((bf16[2,384,2048]{1,0,2:T(2,128)(2,1)}), bf16[2,384,2048]{1,0,2:T(2,128)(2,1)S(1)}, u32[]{:S(2)}, u32[]{:S(2)}) async-start(bf16[2,384,2048]{1,0,2:T(2,128)(2,1)} %copy.35), calls=%async_computation.2 | async-start | bytes 6291456 | tf_op jit(solution)/shard_map/all_to_all | solution.py:61
  199.0 102.2 %all-gather.9.cloned.1.call-start = ((), (), s32[]{:S(2)}) async-start(), calls=%async_computation.7 | async-start | bytes 4718592 | tf_op jit(solution)/shard_map/all_gather | solution.py:77
  235.9 15.9 %all-to-all-start.4 = ((bf16[4,192,512]{2,1,0:T(8,128)(2,1)}), bf16[4,192,512]{2,1,0:T(8,128)(2,1)}, u32[]{:S(2)}, u32[]{:S(2)}) async-start(bf16[4,192,512]{2,1,0:T(8,128)(2,1)} %bitcast.74), calls=%async_computation.4 | async-start | bytes 1572864 | tf_op jit(solution)/shard_map/all_to_all | solution.py:69
  251.7 92.3 %all-to-all-start.3 = ((bf16[8,384,512]{2,1,0:T(8,128)(2,1)}), bf16[8,384,512]{2,1,0:T(8,128)(2,1)S(1)}, u32[]{:S(2)}, u32[]{:S(2)}) async-start(bf16[8,384,512]{2,1,0:T(8,128)(2,1)} %bitcast.70), calls=%async_computation.3 | async-start | bytes 6291456 | tf_op jit(solution)/shard_map/all_to_all | solution.py:11
  308.2 40.2 %copy-start.7 = (f32[512]{0:T(512)S(1)}, f32[512]{0:T(512)}, u32[]{:S(2)}) copy-start(f32[512]{0:T(512)} %param.19) | copy-start | bytes 6148
  308.2 40.8 %copy-start.5 = (f32[768,2]{0,1:T(2,128)S(1)}, f32[768,2]{0,1:T(2,128)}, u32[]{:S(2)}) copy-start(f32[768,2]{0,1:T(2,128)} %param.13) | copy-start | bytes 18436
  344.0 20.0 %all-to-all-start.6 = ((bf16[192,4,512]{2,0,1:T(8,128)(2,1)}), bf16[192,4,512]{2,0,1:T(8,128)(2,1)}, u32[]{:S(2)}, u32[]{:S(2)}) async-start(bf16[192,4,512]{2,0,1:T(8,128)(2,1)} %bitcast.78), calls=%async_computation.6 | async-start | bytes 1572864 | tf_op jit(solution)/shard_map/all_to_all | solution.py:86
  358.1 5.9 %copy-start.4 = (f32[512]{0:T(512)S(1)}, f32[512]{0:T(512)}, u32[]{:S(2)}) copy-start(f32[512]{0:T(512)} %add_divide_fusion) | copy-start | bytes 6148
Sparse Core Ops, SparseCore 0:
  8.9 25.2 all-gather.12
  35.8 23.4 all-gather.14
  60.9 23.6 all-gather.16
  86.4 92.0 all-gather.10
  201.5 99.6 all-gather.8
